TPU v7x, 32 devices: a whole 2x2x4 slice. The times are simulated.
32 devices in a mesh: grp: 2 (over x), ep: 16 (over z, y, core).
Axes of the slice: x: 2, y: 2, z: 4, core: 2. Of those that a mesh axis runs over, the one named last changes fastest.
Arguments:
- tokens: bfloat16 [512, 2048], P(('grp', 'ep')), parts along dimension 0, may hold values from -6 to 6
- attn_gain: float32 [2048], replicated, may hold values from 0.1 to 1.9
- w_query: bfloat16 [2048, 1024], replicated, may hold values from -0.125 to 0.125
- w_key: bfloat16 [2048, 128], replicated, may hold values from -0.125 to 0.125
- w_value: bfloat16 [2048, 128], replicated, may hold values from -0.125 to 0.125
- w_forget: bfloat16 [2048, 2], replicated, may hold values from -0.125 to 0.125
- forget_bias: float32 [2], replicated, may hold values from -3 to 1
- w_attn_out: bfloat16 [1024, 2048], replicated, may hold values from -0.1875 to 0.1875
- cache_keys: bfloat16 [512, 1024, 128], P(('grp', 'ep')), parts along dimension 0, may hold values from -640 to 640
- cache_values: bfloat16 [512, 1024, 128], P(('grp', 'ep')), parts along dimension 0, may hold values from -6 to 6
- cache_logsum: float32 [512, 2, 1024], P(('grp', 'ep')), parts along dimension 0, may hold values from -100 to 0, as said below
- lengths: int32 [512], P(('grp', 'ep')), parts along dimension 0, may hold values from 1 to 1024, as said below
- ffn_gain: float32 [2048], replicated, may hold values from 0.1 to 1.9
- branch_gate: float32 [2048], replicated, may hold values from -0.125 to 0.125
- dense_gate: bfloat16 [2048, 4096], P(None, 'ep'), may hold values from -0.125 to 0.125
- dense_up: bfloat16 [2048, 4096], P(None, 'ep'), may hold values from -0.125 to 0.125
- dense_down: bfloat16 [4096, 2048], P('ep'), may hold values from -0.09375 to 0.09375
- expert_gate: bfloat16 [16, 2048, 512], P('ep'), may hold values from -0.125 to 0.125
- expert_up: bfloat16 [16, 2048, 512], P('ep'), may hold values from -0.125 to 0.125
- expert_down: bfloat16 [16, 512, 2048], P('ep'), may hold values from -0.25 to 0.25
- routes: int32 [512, 4], P(('grp', 'ep')), parts along dimension 0, may hold values from 0 to 15, all different within a row; in each aligned block of 16 rows (0 to 15, 16 to 31, ...) at most 8 rows name the same one
- route_weights: float32 [512, 4], P(('grp', 'ep')), parts along dimension 0, may hold values from 0.2 to 1
Outputs:
- output_rows: bfloat16 [512, 2048], P(('grp', 'ep')), parts along dimension 0
There are 2 independent parts, one for each index of `grp`. A program takes and returns all parts, laid end to end along the dimension named above; an argument that names none is the same for every part. Nothing has to cross between parts.
Inputs may be any that keep to these rules, and one draw needn't show every extreme that they name: `lengths`: each aligned block of 16 sequences holds one with 1024 valid positions; every length is at least 128. `routes`: a row's 4 experts differ; among the rows of one device no expert is named more than 8 times. `cache_logsum`: non-increasing along positions.
All inputs are finite; a program needn't handle non-finite values.
Results may differ from a plain program's by a relative error of at most 0.012.
The roundings to bfloat16 on the way count: a program that leaves them out, or rounds other values in their place, can miss the bound.
Values may be sent and summed in bfloat16 or wider, within the bound.
A program may use at most 128 MiB of HBM per device.

v0:
```python
import math

import jax
import jax.numpy as jnp
from jax import lax
from jax.sharding import PartitionSpec as P

EPSILON = 1e-06


def norm_rows(inputs, gain_vec):
    widened = inputs.astype(jnp.float32)
    scaled = widened * lax.rsqrt(jnp.mean(widened * widened, axis=-1, keepdims=True) + EPSILON)
    return (scaled * gain_vec).astype(jnp.bfloat16)


def swiglu(row_block, w_first, w_second):
    gate_part = jnp.dot(row_block, w_first, preferred_element_type=jnp.float32)
    up_part = jnp.dot(row_block, w_second, preferred_element_type=jnp.float32)
    return (jax.nn.silu(gate_part) * up_part).astype(jnp.bfloat16)


def expert_rows(row_block, w_gate, w_up, w_down):
    middle = swiglu(row_block, w_gate, w_up)
    return jnp.dot(middle, w_down, preferred_element_type=jnp.float32).astype(jnp.bfloat16)


def attend(
    normed,
    w_query,
    w_key,
    w_value,
    w_forget,
    forget_bias,
    cache_keys,
    cache_values,
    cache_logsum,
    lengths,
):
    own_rows = normed.shape[0]
    kv_heads = cache_logsum.shape[1]
    cache_span = cache_logsum.shape[2]
    head_size = w_key.shape[1] // kv_heads
    group_size = w_query.shape[1] // head_size // kv_heads
    scaling = 1.0 / math.sqrt(head_size)
    queries = jnp.dot(normed, w_query, preferred_element_type=jnp.float32).astype(jnp.bfloat16)
    new_keys = jnp.dot(normed, w_key, preferred_element_type=jnp.float32).astype(jnp.bfloat16)
    new_values = jnp.dot(normed, w_value, preferred_element_type=jnp.float32).astype(jnp.bfloat16)
    log_gate = jax.nn.log_sigmoid(
        jnp.dot(normed, w_forget, preferred_element_type=jnp.float32) + forget_bias
    )
    positions = lax.broadcasted_iota(jnp.int32, (own_rows, kv_heads, cache_span), 2)
    latest = jnp.sum(jnp.where(positions == lengths[:, None, None] - 1, cache_logsum, 0.0), axis=2)
    offsets = (latest + log_gate)[:, :, None] - cache_logsum
    usable = positions < lengths[:, None, None]
    query_heads = queries.reshape(own_rows, kv_heads, group_size, head_size)
    key_heads = cache_keys.reshape(own_rows, cache_span, kv_heads, head_size)
    value_heads = cache_values.reshape(own_rows, cache_span, kv_heads, head_size)
    scores = (
        jnp.einsum("bgrd,blgd->bgrl", query_heads, key_heads, preferred_element_type=jnp.float32)
        * scaling
    )
    scores = jnp.where(usable[:, :, None, :], scores + offsets[:, :, None, :], -jnp.inf)
    self_score = (
        jnp.einsum(
            "bgrd,bgd->bgr",
            query_heads,
            new_keys.reshape(own_rows, kv_heads, head_size),
            preferred_element_type=jnp.float32,
        )
        * scaling
    )
    peak_score = jnp.maximum(jnp.max(scores, axis=3), self_score)
    cache_weight = jnp.exp(scores - peak_score[..., None])
    self_weight = jnp.exp(self_score - peak_score)
    denominator = jnp.sum(cache_weight, axis=3) + self_weight
    cache_probs = (cache_weight / denominator[..., None]).astype(jnp.bfloat16)
    self_probs = (self_weight / denominator).astype(jnp.bfloat16)
    attended = jnp.einsum(
        "bgrl,blgd->bgrd", cache_probs, value_heads, preferred_element_type=jnp.float32
    )
    attended = attended + self_probs.astype(jnp.float32)[..., None] * new_values.reshape(
        own_rows, kv_heads, 1, head_size
    ).astype(jnp.float32)
    return attended.reshape(own_rows, -1).astype(jnp.bfloat16)


def body(
    tokens,
    attn_gain,
    w_query,
    w_key,
    w_value,
    w_forget,
    forget_bias,
    w_attn_out,
    cache_keys,
    cache_values,
    cache_logsum,
    lengths,
    ffn_gain,
    branch_gate,
    dense_gate,
    dense_up,
    dense_down,
    expert_gate,
    expert_up,
    expert_down,
    routes,
    route_weights,
):
    own_rows = tokens.shape[0]
    normed = norm_rows(tokens, attn_gain)
    attended = attend(
        normed,
        w_query,
        w_key,
        w_value,
        w_forget,
        forget_bias,
        cache_keys,
        cache_values,
        cache_logsum,
        lengths,
    )
    residual = tokens.astype(jnp.float32) + jnp.dot(
        attended, w_attn_out, preferred_element_type=jnp.float32
    )
    second = norm_rows(residual, ffn_gain)
    branch_share = jax.nn.sigmoid(
        jnp.dot(second.astype(jnp.float32), branch_gate, precision=lax.Precision.HIGHEST)
    )
    expert_count = lax.axis_size("ep")
    route_count = routes.shape[1]
    capacity = max(2, 2 * own_rows * route_count // expert_count)
    hits = (
        routes[:, :, None]
        == lax.broadcasted_iota(jnp.int32, (own_rows, route_count, expert_count), 2)
    ).astype(jnp.int32)
    flat_hits = hits.reshape(own_rows * route_count, expert_count)
    order_rank = jnp.sum((jnp.cumsum(flat_hits, axis=0) - 1) * flat_hits, axis=1).reshape(
        own_rows, route_count
    )
    slot_index = routes * capacity + order_rank
    slot_total = expert_count * capacity
    matches = slot_index[None, :, :] == lax.broadcasted_iota(
        jnp.int32, (slot_total, own_rows, route_count), 0
    )
    dispatch = jnp.sum(matches.astype(jnp.float32), axis=2).astype(jnp.bfloat16)
    combine = jnp.sum(jnp.where(matches, route_weights[None, :, :], 0.0), axis=2).T
    outgoing = jnp.dot(dispatch, second, preferred_element_type=jnp.float32).astype(jnp.bfloat16)
    outgoing = outgoing.reshape(expert_count, 1, capacity, -1)
    arrived = lax.all_to_all(outgoing, "ep", split_axis=0, concat_axis=1, tiled=True)
    arrived_shape = arrived.shape
    answer = expert_rows(
        arrived.reshape(-1, arrived_shape[3]), expert_gate[0], expert_up[0], expert_down[0]
    )
    returned = lax.all_to_all(
        answer.reshape(arrived_shape), "ep", split_axis=1, concat_axis=0, tiled=True
    )
    routed = jnp.dot(
        combine,
        returned.reshape(slot_total, -1).astype(jnp.float32),
        precision=lax.Precision.HIGHEST,
    )
    dense_hidden = swiglu(lax.all_gather(second, "ep", axis=0, tiled=True), dense_gate, dense_up)
    dense = lax.psum_scatter(
        jnp.dot(dense_hidden, dense_down, preferred_element_type=jnp.float32).astype(jnp.bfloat16),
        "ep",
        scatter_dimension=0,
        tiled=True,
    ).astype(jnp.float32)
    output_rows = residual + branch_share[:, None] * dense + routed
    return output_rows.astype(jnp.bfloat16)


def solution(mesh):
    return jax.shard_map(
        body,
        mesh=mesh,
        in_specs=(
            P(("grp", "ep"), None),
            P(),
            P(),
            P(),
            P(),
            P(),
            P(),
            P(),
            P(("grp", "ep"), None, None),
            P(("grp", "ep"), None, None),
            P(("grp", "ep"), None, None),
            P(("grp", "ep")),
            P(),
            P(),
            P(None, "ep"),
            P(None, "ep"),
            P("ep", None),
            P("ep", None, None),
            P("ep", None, None),
            P("ep", None, None),
            P(("grp", "ep"), None),
            P(("grp", "ep"), None),
        ),
        out_specs=P(("grp", "ep"), None),
        check_vma=False,
    )
```

profile of v0, /device:TPU:0, one launch (start us, length us, event | category | flops | bytes accessed | tf_op | source)
XLA Modules:
  0.0 152.9 jit_solution(14952245672474803569)
XLA Ops:
  6.6 0.8 broadcast_add_fusion
  7.4 0.8 iota_compare_fusion
  8.2 1.0 fusion.43
  9.2 2.9 %convolution_convert_fusion.3 = bf16[16,1024]{1,0:T(8,128)(2,1)S(1)} fusion(bf16[2048,1024]{1,0:T(8,128)(2,1)} %param.24, bf16[16,2048]{1,0:T(8,128)(2,1)} %param.22, f32[2048]{0:T(1024)} %param.23, f32[16]{0:T(128)S(1)} %add_rsqrt_fusion.1), kind=kOutput, calls=%fused_computation.22 | convolution fusion | flops 67256320 | bytes 4300864 | tf_op jit(solution)/shard_map/dot_general | solution.py:46
  12.1 0.1 reshape.95
  12.3 0.2 fusion.46
  12.6 0.2 fusion.53
  12.9 0.1 broadcast_subtract_fusion
  13.0 6.5 %copy.53 = bf16[16,1024,128]{1,2,0:T(8,128)(2,1)} copy(bf16[16,1024,128]{2,1,0:T(8,128)(2,1)} %param.30) | data formatting | bytes 8388608 | tf_op args[8]
  19.5 0.2 convolution_convert_fusion.5
  19.8 0.2 fusion.62
  20.0 3.0 %fusion.61 = (f32[16,2,8]{2,1,0:T(2,128)S(1)}, f32[16,2,8,1024]{3,2,1,0:T(8,128)S(1)}) fusion(f32[16,2,1024]{2,1,0:T(2,128)S(1)} %broadcast_subtract_fusion, bf16[16,2,8,64]{3,2,1,0:T(8,128)(2,1)S(1)} %reshape.95, bf16[16,1024,2,64]{1,3,2,0:T(8,128)(2,1)} %bitcast.70, pred[16,2,1024]{2,1,0:T(4,128)(4,1)S(1)} %iota_compare_fusion), kind=kOutput, calls=%fused_computation.85 | convolution fusion | flops 34602752 | bytes 5440512 | tf_op jit(solution)/shard_map/bgrd,blgd->bgrl/dot_general | solution.py:60
  23.0 0.3 fusion.24
  23.3 1.3 fusion.18
  24.7 6.4 %copy.56 = bf16[16,1024,128]{1,2,0:T(8,128)(2,1)} copy(bf16[16,1024,128]{2,1,0:T(8,128)(2,1)} %param.31) | data formatting | bytes 8388608 | tf_op args[9]
  31.1 3.4 %fusion.17 = bf16[16,2,8,64]{3,2,1,0:T(8,128)(2,1)S(1)} fusion(bf16[16,1024,2,64]{1,3,2,0:T(8,128)(2,1)} %bitcast.71, f32[16,2,8,1024]{3,2,1,0:T(8,128)S(1)} %get-tuple-element.10, f32[16,2,8]{2,1,0:T(2,128)S(1)} %get-tuple-element.8, f32[16,2,8]{2,1,0:T(2,128)S(1)} %multiply_maximum_fusion, f32[16,2,64]{2,1,0:T(2,128)S(1)} %reshape.103, ...), kind=kOutput, calls=%fused_computation.21 | convolution fusion | flops 34390016 | bytes 5286912 | tf_op jit(solution)/shard_map/bgrl,blgd->bgrd/dot_general | solution.py:79
  34.5 0.1 convert_element_type.90
  34.7 3.0 %multiply_reduce_fusion = (f32[16]{0:T(128)S(1)}, f32[16,2048]{1,0:T(8,128)S(1)}) fusion(bf16[16,1024]{1,0:T(8,128)(2,1)S(1)} %convert_element_type.90, bf16[1024,2048]{1,0:T(8,128)(2,1)} %param.29, bf16[16,2048]{1,0:T(8,128)(2,1)S(1)} %copy-done.1), kind=kOutput, calls=%fused_computation.61 | convolution fusion | flops 67239920 | bytes 4423744 | tf_op jit(solution)/shard_map/dot_general | solution.py:126
  37.7 0.7 multiply_convert_fusion
  38.8 0.2 select_reduce_fusion.1
  39.2 2.0 %fusion = bf16[16,1,8,2048]{3,2,1,0:T(8,128)(2,1)} fusion(bf16[16,2048]{1,0:T(8,128)(2,1)} %multiply_convert_fusion, bf16[128,16]{0,1:T(8,128)(2,1)S(1)} %get-tuple-element.5), kind=kOutput, calls=%fused_computation.3 | convolution fusion | flops 8650752 | bytes 593920 | tf_op jit(solution)/shard_map/dot_general | solution.py:151
  41.2 7.4 %all-to-all-start = ((bf16[16,1,8,2048]{3,2,1,0:T(8,128)(2,1)}), bf16[16,1,8,2048]{3,2,1,0:T(8,128)(2,1)S(1)}, u32[]{:S(2)}, u32[]{:S(2)}) async-start(bf16[16,1,8,2048]{3,2,1,0:T(8,128)(2,1)} %fusion), calls=%async_computation.1 | async-start | bytes 1048576 | tf_op jit(solution)/shard_map/all_to_all | solution.py:153
  48.6 32.8 %all-gather.2.cloned.1.call-done = bf16[256,2048]{1,0:T(8,128)(2,1)} async-done(((bf16[16,2048]{1,0:T(8,128)(2,1)}), bf16[256,2048]{1,0:T(8,128)(2,1)}) %all-gather.2.cloned.1.call-update) | async-done | bytes 1048592 | tf_op jit(solution)/shard_map/all_gather | solution.py:166
  81.5 2.0 %fusion.63 = f32[256,256]{1,0:T(8,128)S(1)} fusion(bf16[256,2048]{1,0:T(8,128)(2,1)} %all-gather.2.cloned.1.call-done, bf16[2048,256]{1,0:T(8,128)(2,1)} %param.36), kind=kOutput, calls=%fused_computation.87 | convolution fusion | flops 268435456 | bytes 2359296 | tf_op jit(solution)/shard_map/dot_general | solution.py:18
  83.4 4.1 %convolution_convert_fusion = bf16[256,2048]{1,0:T(8,128)(2,1)} fusion(bf16[256,2048]{1,0:T(8,128)(2,1)} %param.38, bf16[256,2048]{1,0:T(8,128)(2,1)} %all-gather.2.cloned.1.call-done, bf16[2048,256]{1,0:T(8,128)(2,1)} %param.37, f32[256,256]{1,0:T(8,128)S(1)} %fusion.63), kind=kOutput, calls=%fused_computation | convolution fusion | flops 537788416 | bytes 4456448 | tf_op jit(solution)/shard_map/dot_general | solution.py:168
  87.6 2.0 %fusion.6 = f32[128,512]{1,0:T(8,128)S(1)} fusion(bf16[1,2048,512]{2,1,0:T(8,128)(2,1)} %param.39, bf16[16,1,8,2048]{3,2,1,0:T(8,128)(2,1)S(1)} %all-to-all-done), kind=kOutput, calls=%fused_computation.11 | convolution fusion | flops 268435456 | bytes 2883584 | tf_op jit(solution)/shard_map/dot_general | solution.py:18
  89.7 3.2 %fusion.1 = bf16[1,16,8,2048]{3,2,0,1:T(8,128)(2,1)} fusion(bf16[1,512,2048]{2,1,0:T(8,128)(2,1)S(1)} %copy-done, bf16[1,2048,512]{2,1,0:T(8,128)(2,1)} %param.40, bf16[16,1,8,2048]{3,2,1,0:T(8,128)(2,1)S(1)} %all-to-all-done, f32[128,512]{1,0:T(8,128)S(1)} %fusion.6), kind=kOutput, calls=%fused_computation.4 | convolution fusion | flops 537526272 | bytes 5505024 | tf_op jit(solution)/shard_map/dot_general | solution.py:25
  92.9 3.7 %all-to-all-start.1 = ((bf16[1,16,8,2048]{3,2,0,1:T(8,128)(2,1)}), bf16[1,16,8,2048]{3,2,0,1:T(8,128)(2,1)S(1)}, u32[]{:S(2)}, u32[]{:S(2)}) async-start(bf16[1,16,8,2048]{3,2,0,1:T(8,128)(2,1)} %fusion.1), calls=%async_computation.2 | async-start | bytes 1048576 | tf_op jit(solution)/shard_map/all_to_all | solution.py:158
  96.7 0.1 fusion.23
  96.8 14.1 %all-to-all-done.1 = bf16[1,16,8,2048]{3,2,0,1:T(8,128)(2,1)S(1)} async-done(((bf16[1,16,8,2048]{3,2,0,1:T(8,128)(2,1)}), bf16[1,16,8,2048]{3,2,0,1:T(8,128)(2,1)S(1)}, u32[]{:S(2)}, u32[]{:S(2)}) %all-to-all-start.1) | async-done | bytes 524320 | tf_op jit(solution)/shard_map/all_to_all | solution.py:158
  110.9 33.4 %reduce-scatter.2.cloned.1.call-done = bf16[16,2048]{1,0:T(8,128)(2,1)} async-done(((bf16[256,2048]{1,0:T(8,128)(2,1)}), bf16[16,2048]{1,0:T(8,128)(2,1)}) %reduce-scatter.2.cloned.1.call-update) | async-done | bytes 65552 | tf_op jit(solution)/shard_map/reduce_scatter | solution.py:167
  144.3 1.8 %fusion.2 = bf16[16,2048]{1,0:T(8,128)(2,1)} fusion(f32[128,16]{0,1:T(8,128)S(1)} %get-tuple-element.6, bf16[1,16,8,2048]{3,2,0,1:T(8,128)(2,1)S(1)} %all-to-all-done.1, f32[16,2048]{1,0:T(8,128)S(1)} %get-tuple-element.12, bf16[16,2048]{1,0:T(8,128)(2,1)} %reduce-scatter.2.cloned.1.call-done, f32[16]{0:T(128)S(1)} %fusion.23), kind=kOutput, calls=%fused_computation.7 | convolution fusion | flops 50495488 | bytes 794688 | tf_op jit(solution)/shard_map/dot_general | solution.py:161
  (45 shorter events, 1.2 us)
Async XLA Ops:
  6.5 83.2 %copy-start = (bf16[1,512,2048]{2,1,0:T(8,128)(2,1)S(1)}, bf16[1,512,2048]{2,1,0:T(8,128)(2,1)}, u32[]{:S(2)}) copy-start(bf16[1,512,2048]{2,1,0:T(8,128)(2,1)} %param.41) | copy-start | bytes 6291460
  6.5 6.0 %copy-start.1 = (bf16[16,2048]{1,0:T(8,128)(2,1)S(1)}, bf16[16,2048]{1,0:T(8,128)(2,1)}, u32[]{:S(2)}) copy-start(bf16[16,2048]{1,0:T(8,128)(2,1)} %param.22) | copy-start | bytes 196612
  6.5 6.0 %copy-start.5 = (f32[2048]{0:T(1024)S(1)}, f32[2048]{0:T(1024)}, u32[]{:S(2)}) copy-start(f32[2048]{0:T(1024)} %param.23) | copy-start | bytes 24580
  6.5 5.7 %copy-start.4 = (f32[16,2,1024]{2,1,0:T(2,128)S(1)}, f32[16,2,1024]{2,1,0:T(2,128)}, u32[]{:S(2)}) copy-start(f32[16,2,1024]{2,1,0:T(2,128)} %param.32) | copy-start | bytes 393220
  6.5 6.0 %copy-start.9 = (bf16[2048,2]{0,1:T(2,128)(2,1)S(1)}, bf16[2048,2]{0,1:T(2,128)(2,1)}, u32[]{:S(2)}) copy-start(bf16[2048,2]{0,1:T(2,128)(2,1)} %param.27) | copy-start | bytes 24580
  6.5 6.0 %copy-start.11 = (f32[2]{0:T(128)S(1)}, f32[2]{0:T(128)}, u32[]{:S(2)}) copy-start(f32[2]{0:T(128)} %param.28) | copy-start | bytes 28
  6.6 74.9 %all-gather.2.cloned.1.call-start = ((), (), s32[]{:S(2)}) async-start(), calls=%async_computation.3 | async-start | bytes 1114112 | tf_op jit(solution)/shard_map/all_gather | solution.py:166
  13.0 6.5 %copy-start.3 = (bf16[2048,128]{1,0:T(8,128)(2,1)S(1)}, bf16[2048,128]{1,0:T(8,128)(2,1)}, u32[]{:S(2)}) copy-start(bf16[2048,128]{1,0:T(8,128)(2,1)} %param.25) | copy-start | bytes 1572868
  31.1 6.6 %copy-start.6 = (f32[2048]{0:T(1024)S(1)}, f32[2048]{0:T(1024)}, u32[]{:S(2)}) copy-start(f32[2048]{0:T(1024)} %param.34) | copy-start | bytes 24580
  34.5 3.9 %copy-start.7 = (s32[16,4]{0,1:T(4,128)S(1)}, s32[16,4]{0,1:T(4,128)}, u32[]{:S(2)}) copy-start(s32[16,4]{0,1:T(4,128)} %param.42) | copy-start | bytes 772
  34.5 4.6 %copy-start.8 = (f32[16,4]{0,1:T(4,128)S(1)}, f32[16,4]{0,1:T(4,128)}, u32[]{:S(2)}) copy-start(f32[16,4]{0,1:T(4,128)} %param.43) | copy-start | bytes 772
  41.2 46.4 %all-to-all-start = ((bf16[16,1,8,2048]{3,2,1,0:T(8,128)(2,1)}), bf16[16,1,8,2048]{3,2,1,0:T(8,128)(2,1)S(1)}, u32[]{:S(2)}, u32[]{:S(2)}) async-start(bf16[16,1,8,2048]{3,2,1,0:T(8,128)(2,1)} %fusion), calls=%async_computation.1 | async-start | bytes 1048576 | tf_op jit(solution)/shard_map/all_to_all | solution.py:153
  48.6 95.7 %reduce-scatter.2.cloned.1.call-start = ((), (), s32[]{:S(2)}) async-start(), calls=%async_computation.4 | async-start | bytes 1114112 | tf_op jit(solution)/shard_map/reduce_scatter | solution.py:167
  87.6 9.0 %copy-start.2 = (bf16[16,2048]{1,0:T(8,128)(2,1)S(1)}, bf16[16,2048]{1,0:T(8,128)(2,1)}, u32[]{:S(2)}) copy-start(bf16[16,2048]{1,0:T(8,128)(2,1)} %multiply_convert_fusion) | copy-start | bytes 196612
  87.6 9.0 %copy-start.10 = (f32[2048]{0:T(1024)S(1)}, f32[2048]{0:T(1024)}, u32[]{:S(2)}) copy-start(f32[2048]{0:T(1024)} %param.35) | copy-start | bytes 24580
  92.9 18.0 %all-to-all-start.1 = ((bf16[1,16,8,2048]{3,2,0,1:T(8,128)(2,1)}), bf16[1,16,8,2048]{3,2,0,1:T(8,128)(2,1)S(1)}, u32[]{:S(2)}, u32[]{:S(2)}) async-start(bf16[1,16,8,2048]{3,2,0,1:T(8,128)(2,1)} %fusion.1), calls=%async_computation.2 | async-start | bytes 1048576 | tf_op jit(solution)/shard_map/all_to_all | solution.py:158
Sparse Core Ops, SparseCore 0:
  38.5 42.8 all-gather.1
  87.7 56.5 reduce-scatter.1
where the time goes:
time: 154 us; the launch traced here: 153 us
  waiting for transfers between devices  80.4 us (52%)
  matrix products  29.5 us (19%)
  local copies, waits for them, and re-layouts  13.8 us (9%)
  between operations  13.6 us (9%)
  starting transfers between devices  11.2 us (7%)
  other arithmetic  4.46 us (3%)
    reduce_scatter x1, waiting for transfers between devices, body(): lax.psum_scatter(jnp.dot(dense_hidden, dense_down, preferred_element_type...  33.4 us
    all_gather x1, waiting for transfers between devices, body(): lax.all_gather(second, 'ep', axis=0, tiled=True)  32.8 us
    all_to_all x1, waiting for transfers between devices, body(): lax.all_to_all(answer.reshape(arrived_shape), 'ep', split_axis=1, concat_...  14.1 us
    unnamed x27, local copies, waits for them, and re-layouts  13 us
    all_to_all x1, starting transfers between devices, body(): lax.all_to_all(outgoing, 'ep', split_axis=0, concat_axis=1, tiled=True)  7.41 us
    dot_general x1, matrix products, body(): jnp.dot(dense_hidden, dense_down, preferred_element_type=jnp.float32)  4.14 us
    dot_general x2, matrix products, swiglu(): gate_part = jnp.dot(row_block, w_first, preferred_element_type=jnp.float32)  4.02 us
    all_to_all x1, starting transfers between devices, body(): lax.all_to_all(answer.reshape(arrived_shape), 'ep', split_axis=1, concat_...  3.68 us
  transfers between devices with their start and end apart: 4, of which 3 were waited for; matrix products, arithmetic and copies ran while one was open for 9% of the time, Pallas kernels for 0%

commit v1 on v0

--- a/solution.py
+++ b/solution.py
@@ -3,26 +3,259 @@
 import jax
 import jax.numpy as jnp
 from jax import lax
+from jax.experimental import pallas as pl
+from jax.experimental.pallas import tpu as pltpu
 from jax.sharding import PartitionSpec as P
 
 EPSILON = 1e-06
+LANES = 128
+CORES = 2
+SIDES = 2
+CHUNKS = 4
+MESH = pl.DeviceIdType.MESH
+
+
+def exchange_kernel(
+    count,
+    depth,
+    block_ref,
+    residual_ref,
+    branch_ref,
+    dense_gate_hbm,
+    dense_up_hbm,
+    dense_down_hbm,
+    expert_gate_hbm,
+    expert_up_hbm,
+    expert_down_hbm,
+    out_ref,
+    rows_buf,
+    dense_gate,
+    dense_up,
+    dense_down,
+    expert_gate,
+    expert_up,
+    expert_down,
+    partial,
+    core_out,
+    core_in,
+    side_out,
+    side_in,
+    depth_out,
+    depth_in,
+    kept,
+    load_sem,
+    gather_send,
+    gather_recv,
+    scatter_send,
+    scatter_recv,
+):
+    me = lax.axis_index("ep")
+    core = lax.rem(me, CORES)
+    side = lax.rem(me // CORES, SIDES)
+    level = me // (CORES * SIDES)
+    own_rows, width = residual_ref.shape
+    step = width // CHUNKS
+
+    def device(level_at, side_at, core_at):
+        return {"ep": level_at * (CORES * SIDES) + side_at * CORES + core_at}
+
+    def away(distance):
+        return lax.rem(level + distance, depth)
+
+    def behind(distance):
+        return lax.rem(level + depth - distance, depth)
+
+    partner = device(level, side, 1 - core)
+    across = device(level, 1 - side, core)
+
+    loads = [
+        pltpu.make_async_copy(source, target, load_sem.at[at])
+        for at, (source, target) in enumerate(
+            (
+                (dense_gate_hbm, dense_gate),
+                (dense_up_hbm, dense_up),
+                (expert_gate_hbm.at[0], expert_gate),
+                (expert_up_hbm.at[0], expert_up),
+                (dense_down_hbm, dense_down),
+                (expert_down_hbm.at[0], expert_down),
+            )
+        )
+    ]
+    for load in loads:
+        load.start()
+
+    barrier = pltpu.get_barrier_semaphore()
+    for peer in [partner, across] + [device(away(d), side, core) for d in range(1, depth)]:
+        pl.semaphore_signal(barrier, inc=1, device_id=peer, device_id_type=MESH)
+    pl.semaphore_wait(barrier, depth + 1)
+
+    started = []
+
+    def send(source, target, send_sem, recv_sem, peer):
+        copy = pltpu.make_async_remote_copy(
+            src_ref=source,
+            dst_ref=target,
+            send_sem=send_sem,
+            recv_sem=recv_sem,
+            device_id=peer,
+            device_id_type=MESH,
+        )
+        copy.start()
+        started.append(copy)
+
+    def arrive(target, recv_sem):
+        pltpu.make_async_remote_copy(
+            src_ref=target,
+            dst_ref=target,
+            send_sem=recv_sem,
+            recv_sem=recv_sem,
+            device_id=partner,
+            device_id_type=MESH,
+        ).wait_recv()
+
+    side_at = depth - 1
+    core_at = side_at + depth
+    own_slot = rows_buf.at[core, side, level]
+
+    def pass_on(source, slot, at, peer):
+        send(source, slot, gather_send.at[at], gather_recv.at[at], peer)
+
+    for d in range(1, depth):
+        pass_on(block_ref, own_slot, d - 1, device(away(d), side, core))
+    pass_on(block_ref, own_slot, side_at, across)
+    pass_on(block_ref, own_slot, core_at, partner)
+    rows_buf[core, side, level] = block_ref[...]
+    for d in range(1, depth + 1):
+        if d < depth:
+            slot = rows_buf.at[core, side, behind(d)]
+            arrive(slot, gather_recv.at[d - 1])
+            pass_on(slot, slot, side_at + d, across)
+            pass_on(slot, slot, core_at + d, partner)
+        slot = rows_buf.at[core, 1 - side, behind(d - 1)]
+        arrive(slot, gather_recv.at[side_at + d - 1])
+        pass_on(slot, slot, core_at + depth + d - 1, partner)
+    for d in range(depth):
+        arrive(rows_buf.at[1 - core, side, behind(d)], gather_recv.at[core_at + d])
+    for d in range(depth):
+        arrive(rows_buf.at[1 - core, 1 - side, behind(d)], gather_recv.at[core_at + depth + d])
+
+    gathered = rows_buf[...].reshape(count * own_rows, block_ref.shape[1])
+    second = gathered[:, :width]
+    extra = gathered[:, width:].astype(jnp.float32)
+    lane = lax.broadcasted_iota(jnp.int32, extra.shape, 1)
+    mine = (lane == me) | (lane == me + count) | (lane == me + 2 * count)
+    weight = jnp.sum(jnp.where(mine, extra, 0.0), axis=1, keepdims=True)
+    share = jax.nn.sigmoid(
+        jnp.sum(second.astype(jnp.float32) * branch_ref[...], axis=1, keepdims=True)
+    )
+
+    def hidden(gate_ref, up_ref):
+        gate_part = jnp.dot(second, gate_ref[...], preferred_element_type=jnp.float32)
+        up_part = jnp.dot(second, up_ref[...], preferred_element_type=jnp.float32)
+        return (jax.nn.silu(gate_part) * up_part).astype(jnp.bfloat16)
+
+    loads[0].wait()
+    loads[1].wait()
+    dense_hidden = hidden(dense_gate, dense_up)
+    loads[2].wait()
+    loads[3].wait()
+    expert_hidden = hidden(expert_gate, expert_up)
+    loads[4].wait()
+    loads[5].wait()
+
+    def produce(j):
+        columns = pl.ds(j * step, step)
+        dense = jnp.dot(dense_hidden, dense_down[:, columns], preferred_element_type=jnp.float32)
+        answer = jnp.dot(expert_hidden, expert_down[:, columns], preferred_element_type=jnp.float32)
+        total = share * dense + weight * answer.astype(jnp.bfloat16).astype(jnp.float32)
+        partial[j] = total.reshape(partial.shape[1:])
+        core_out[j] = partial[j, 1 - core].astype(jnp.bfloat16)
+        send(core_out.at[j], core_in.at[j], scatter_send.at[j, 0], scatter_recv.at[j, 0], partner)
+
+    def to_side(j):
+        arrive(core_in.at[j], scatter_recv.at[j, 0])
+        other = partial[j, core, 1 - side] + core_in[j, 1 - side].astype(jnp.float32)
+        side_out[j] = other.astype(jnp.bfloat16)
+        send(side_out.at[j], side_in.at[j], scatter_send.at[j, 1], scatter_recv.at[j, 1], across)
+
+    def to_depth(j):
+        arrive(side_in.at[j], scatter_recv.at[j, 1])
+        total = (
+            partial[j, core, side]
+            + core_in[j, side].astype(jnp.float32)
+            + side_in[j].astype(jnp.float32)
+        )
+        kept[j] = total
+        depth_out[j] = total.astype(jnp.bfloat16)
+        for d in range(1, depth):
+            send(
+                depth_out.at[j, away(d)],
+                depth_in.at[j, d - 1],
+                scatter_send.at[j, 1 + d],
+                scatter_recv.at[j, 1 + d],
+                device(away(d), side, core),
+            )
+
+    def finish(j):
+        columns = pl.ds(j * step, step)
+        total = residual_ref[:, columns] + kept[j, level]
+        for d in range(1, depth):
+            arrive(depth_in.at[j, d - 1], scatter_recv.at[j, 1 + d])
+            total = total + depth_in[j, d - 1].astype(jnp.float32)
+        out_ref[:, columns] = total.astype(out_ref.dtype)
+
+    for tick in range(CHUNKS + 3):
+        for delay, stage in ((0, produce), (1, to_side), (2, to_depth), (3, finish)):
+            if 0 <= tick - delay < CHUNKS:
+                stage(tick - delay)
+    for copy in started:
+        copy.wait_send()
+
+
+def exchange(block, residual, branch_gate, *weights):
+    count = lax.axis_size("ep")
+    depth = count // (CORES * SIDES)
+    own_rows, width = residual.shape
+    step = width // CHUNKS
+    wide = block.shape[1]
+    bf16 = jnp.bfloat16
+    grid_rows = (depth, own_rows)
+    gathers = depth - 1 + depth + SIDES * depth
+    scatters = 1 + depth
+    return pl.pallas_call(
+        lambda *refs: exchange_kernel(count, depth, *refs),
+        out_shape=jax.ShapeDtypeStruct((own_rows, width), bf16),
+        in_specs=[pl.BlockSpec(memory_space=pltpu.VMEM)] * 3
+        + [pl.BlockSpec(memory_space=pl.ANY)] * 6,
+        out_specs=pl.BlockSpec(memory_space=pltpu.VMEM),
+        scratch_shapes=[pltpu.VMEM((CORES, SIDES) + grid_rows + (wide,), bf16)]
+        + [pltpu.VMEM(w.shape[-2:], bf16) for w in weights]
+        + [
+            pltpu.VMEM((CHUNKS, CORES, SIDES) + grid_rows + (step,), jnp.float32),
+            pltpu.VMEM((CHUNKS, SIDES) + grid_rows + (step,), bf16),
+            pltpu.VMEM((CHUNKS, SIDES) + grid_rows + (step,), bf16),
+            pltpu.VMEM((CHUNKS,) + grid_rows + (step,), bf16),
+            pltpu.VMEM((CHUNKS,) + grid_rows + (step,), bf16),
+            pltpu.VMEM((CHUNKS,) + grid_rows + (step,), bf16),
+            pltpu.VMEM((CHUNKS, depth - 1, own_rows, step), bf16),
+            pltpu.VMEM((CHUNKS,) + grid_rows + (step,), jnp.float32),
+            pltpu.SemaphoreType.DMA((6,)),
+            pltpu.SemaphoreType.DMA((gathers,)),
+            pltpu.SemaphoreType.DMA((gathers,)),
+            pltpu.SemaphoreType.DMA((CHUNKS, scatters)),
+            pltpu.SemaphoreType.DMA((CHUNKS, scatters)),
+        ],
+        compiler_params=pltpu.CompilerParams(
+            collective_id=0, has_side_effects=True, vmem_limit_bytes=48 * 1024 * 1024
+        ),
+        name="exchange",
+    )(block, residual, branch_gate.reshape(1, -1), *weights)
 
 
 def norm_rows(inputs, gain_vec):
     widened = inputs.astype(jnp.float32)
     scaled = widened * lax.rsqrt(jnp.mean(widened * widened, axis=-1, keepdims=True) + EPSILON)
     return (scaled * gain_vec).astype(jnp.bfloat16)
-
-
-def swiglu(row_block, w_first, w_second):
-    gate_part = jnp.dot(row_block, w_first, preferred_element_type=jnp.float32)
-    up_part = jnp.dot(row_block, w_second, preferred_element_type=jnp.float32)
-    return (jax.nn.silu(gate_part) * up_part).astype(jnp.bfloat16)
-
-
-def expert_rows(row_block, w_gate, w_up, w_down):
-    middle = swiglu(row_block, w_gate, w_up)
-    return jnp.dot(middle, w_down, preferred_element_type=jnp.float32).astype(jnp.bfloat16)
 
 
 def attend(
@@ -127,51 +360,24 @@
         attended, w_attn_out, preferred_element_type=jnp.float32
     )
     second = norm_rows(residual, ffn_gain)
-    branch_share = jax.nn.sigmoid(
-        jnp.dot(second.astype(jnp.float32), branch_gate, precision=lax.Precision.HIGHEST)
-    )
-    expert_count = lax.axis_size("ep")
-    route_count = routes.shape[1]
-    capacity = max(2, 2 * own_rows * route_count // expert_count)
-    hits = (
-        routes[:, :, None]
-        == lax.broadcasted_iota(jnp.int32, (own_rows, route_count, expert_count), 2)
-    ).astype(jnp.int32)
-    flat_hits = hits.reshape(own_rows * route_count, expert_count)
-    order_rank = jnp.sum((jnp.cumsum(flat_hits, axis=0) - 1) * flat_hits, axis=1).reshape(
-        own_rows, route_count
-    )
-    slot_index = routes * capacity + order_rank
-    slot_total = expert_count * capacity
-    matches = slot_index[None, :, :] == lax.broadcasted_iota(
-        jnp.int32, (slot_total, own_rows, route_count), 0
-    )
-    dispatch = jnp.sum(matches.astype(jnp.float32), axis=2).astype(jnp.bfloat16)
-    combine = jnp.sum(jnp.where(matches, route_weights[None, :, :], 0.0), axis=2).T
-    outgoing = jnp.dot(dispatch, second, preferred_element_type=jnp.float32).astype(jnp.bfloat16)
-    outgoing = outgoing.reshape(expert_count, 1, capacity, -1)
-    arrived = lax.all_to_all(outgoing, "ep", split_axis=0, concat_axis=1, tiled=True)
-    arrived_shape = arrived.shape
-    answer = expert_rows(
-        arrived.reshape(-1, arrived_shape[3]), expert_gate[0], expert_up[0], expert_down[0]
-    )
-    returned = lax.all_to_all(
-        answer.reshape(arrived_shape), "ep", split_axis=1, concat_axis=0, tiled=True
-    )
-    routed = jnp.dot(
-        combine,
-        returned.reshape(slot_total, -1).astype(jnp.float32),
-        precision=lax.Precision.HIGHEST,
-    )
-    dense_hidden = swiglu(lax.all_gather(second, "ep", axis=0, tiled=True), dense_gate, dense_up)
-    dense = lax.psum_scatter(
-        jnp.dot(dense_hidden, dense_down, preferred_element_type=jnp.float32).astype(jnp.bfloat16),
-        "ep",
-        scatter_dimension=0,
-        tiled=True,
-    ).astype(jnp.float32)
-    output_rows = residual + branch_share[:, None] * dense + routed
-    return output_rows.astype(jnp.bfloat16)
+    count = lax.axis_size("ep")
+    routed_to = routes[:, :, None] == lax.broadcasted_iota(jnp.int32, routes.shape + (count,), 2)
+    table = jnp.sum(jnp.where(routed_to, route_weights[:, :, None], 0.0), axis=1)
+    high = lax.reduce_precision(table, 8, 7)
+    middle = lax.reduce_precision(table - high, 8, 7)
+    extra = jnp.concatenate([high, middle, table - high - middle], axis=1)
+    extra = jnp.pad(extra, ((0, 0), (0, -extra.shape[1] % LANES))).astype(jnp.bfloat16)
+    return exchange(
+        jnp.concatenate([second, extra], axis=1),
+        residual,
+        branch_gate,
+        dense_gate,
+        dense_up,
+        dense_down,
+        expert_gate,
+        expert_up,
+        expert_down,
+    )
 
 
 def solution(mesh):

time: 154 us -> 68.8 us (0.45)
  waiting for transfers between devices: 80.4 us -> 0 us
  Pallas kernels: 0 us -> 37.2 us
  matrix products: 29.5 us -> 13.4 us
  between operations: 13.6 us -> 0.25 us
  starting transfers between devices: 11.2 us -> 0 us
  other arithmetic: 4.46 us -> 2.16 us
    pallas_call x0 -> x1, Pallas kernels: none -> 37.2 us  [exchange(): pl.pallas_call(lambda *refs: exchange_kernel(count, depth, *refs), out_sh...]
    reduce_scatter x1 -> x0, waiting for transfers between devices: 33.4 us -> none  [body(): lax.psum_scatter(jnp.dot(dense_hidden, dense_down, preferred_element_type...]
    all_gather x1 -> x0, waiting for transfers between devices: 32.8 us -> none  [body(): lax.all_gather(second, 'ep', axis=0, tiled=True)]
    dot_general x7 -> x0, matrix products: 15.3 us -> none  [the longest x1 4.14 us: body(): jnp.dot(dense_hidden, dense_down, preferred_element_type=jnp.float32)]
    all_to_all x2 -> x0, waiting for transfers between devices: 14.1 us -> none  [the longest x1 14.1 us: body(): lax.all_to_all(answer.reshape(arrived_shape), 'ep', split_axis=1, concat_...]
    all_to_all x2 -> x0, starting transfers between devices: 11.1 us -> none  [the longest x1 7.41 us: body(): lax.all_to_all(outgoing, 'ep', split_axis=0, concat_axis=1, tiled=True)]
    unnamed x27 -> x35, local copies, waits for them, and re-layouts: 13 us -> 14.7 us
  transfers between devices with their start and end apart: 4 -> 0, of which waited for: 3 -> 0; matrix products, arithmetic and copies ran while one was open for 9% -> 0% of each run, Pallas kernels for 0% -> 0%
where the time goes in v1:
time: 68.8 us; the launch traced here: 68.3 us
  Pallas kernels  37.2 us (54%)
  local copies, waits for them, and re-layouts  15.3 us (22%)
  matrix products  13.4 us (19%)
  other arithmetic  2.16 us (3%)
    pallas_call x1, Pallas kernels, exchange(): pl.pallas_call(lambda *refs: exchange_kernel(count, depth, *refs), out_sh...  37.2 us
    unnamed x35, local copies, waits for them, and re-layouts  14.7 us
    dot_general x1, matrix products, attend(): jnp.einsum('bgrl,blgd->bgrd', cache_probs, value_heads, preferred_element...  3.48 us
    dot_general x1, matrix products, body(): jnp.dot(attended, w_attn_out, preferred_element_type=jnp.float32)  3.11 us
    dot_general x1, matrix products, attend(): jnp.einsum('bgrd,blgd->bgrl', query_heads, key_heads, preferred_element_t...  2.99 us
    dot_general x1, matrix products, attend(): jnp.dot(normed, w_query, preferred_element_type=jnp.float32)  2.94 us

profile of v1, /device:TPU:0, one launch (start us, length us, event | category | flops | bytes accessed | tf_op | source)
XLA Modules:
  0.0 68.3 jit_solution(16357300318775014560)
XLA Ops:
  0.0 0.0 copy-start
  0.0 0.0 copy-start.8
  0.0 1.0 %fusion.8 = f32[16]{0:T(128)S(1)} fusion(bf16[16,2048]{1,0:T(8,128)(2,1)} %param.22), kind=kLoop, calls=%fused_computation.20 | loop fusion | flops 98288 | bytes 65600 | tf_op jit(solution)/shard_map/reduce_sum | solution.py:257
  1.1 2.9 %convolution_convert_fusion = bf16[16,1024]{1,0:T(8,128)(2,1)S(1)} fusion(bf16[2048,1024]{1,0:T(8,128)(2,1)} %param.24, bf16[16,2048]{1,0:T(8,128)(2,1)} %param.22, f32[2048]{0:T(1024)} %param.23, f32[16]{0:T(128)S(1)} %add_rsqrt_fusion.1), kind=kOutput, calls=%fused_computation.6 | convolution fusion | flops 67256320 | bytes 4300864 | tf_op jit(solution)/shard_map/dot_general | solution.py:279
  4.0 0.1 reshape.60
  4.2 0.2 fusion.11
  4.4 0.1 copy.40
  4.5 0.2 fusion.20
  4.7 0.1 copy.41
  4.8 0.1 broadcast_subtract_fusion
  4.9 6.4 %copy.39 = bf16[16,1024,128]{1,2,0:T(8,128)(2,1)} copy(bf16[16,1024,128]{2,1,0:T(8,128)(2,1)} %param.30) | data formatting | bytes 8388608 | tf_op args[8]
  11.3 0.1 iota_compare_fusion
  11.5 3.0 %fusion.26 = (f32[16,2,8]{2,1,0:T(2,128)S(1)}, f32[16,2,8,1024]{3,2,1,0:T(8,128)S(1)}) fusion(f32[16,2,1024]{2,1,0:T(2,128)S(1)} %broadcast_subtract_fusion, bf16[16,2,8,64]{3,2,1,0:T(8,128)(2,1)S(1)} %reshape.60, bf16[16,1024,2,64]{1,3,2,0:T(8,128)(2,1)} %bitcast.19, pred[16,2,1024]{2,1,0:T(4,128)(4,1)S(1)} %iota_compare_fusion), kind=kOutput, calls=%fused_computation.53 | convolution fusion | flops 34602752 | bytes 5440512 | tf_op jit(solution)/shard_map/bgrd,blgd->bgrl/dot_general | solution.py:293
  14.5 0.2 convolution_convert_fusion.2
  14.7 0.1 reshape.69
  14.8 0.2 fusion.27
  15.0 0.3 fusion.5
  15.4 0.2 fusion.3
  15.6 0.1 reshape.65
  15.7 6.4 %copy.42 = bf16[16,1024,128]{1,2,0:T(8,128)(2,1)} copy(bf16[16,1024,128]{2,1,0:T(8,128)(2,1)} %param.31) | data formatting | bytes 8388608 | tf_op args[9]
  22.1 3.5 %fusion.2 = bf16[16,2,8,64]{3,2,1,0:T(8,128)(2,1)S(1)} fusion(bf16[16,1024,2,64]{1,3,2,0:T(8,128)(2,1)} %bitcast.20, f32[16,2,8,1024]{3,2,1,0:T(8,128)S(1)} %get-tuple-element.11, f32[16,2,8]{2,1,0:T(2,128)S(1)} %get-tuple-element.6, f32[16,2,8]{2,1,0:T(2,128)S(1)} %multiply_maximum_fusion, f32[16,2,64]{2,1,0:T(2,128)S(1)} %reshape.65, ...), kind=kOutput, calls=%fused_computation.5 | convolution fusion | flops 34390016 | bytes 5286912 | tf_op jit(solution)/shard_map/bgrl,blgd->bgrd/dot_general | solution.py:312
  25.6 0.1 convert_element_type.59
  25.7 0.0 copy-start.2
  25.7 0.0 copy-start.3
  25.7 3.1 %multiply_reduce_fusion = (f32[16]{0:T(128)S(1)}, f32[16,2048]{1,0:T(8,128)S(1)}) fusion(bf16[16,1024]{1,0:T(8,128)(2,1)S(1)} %convert_element_type.59, bf16[1024,2048]{1,0:T(8,128)(2,1)} %param.29, bf16[16,2048]{1,0:T(8,128)(2,1)S(1)} %copy-done.6), kind=kOutput, calls=%fused_computation.25 | convolution fusion | flops 67239920 | bytes 4423744 | tf_op jit(solution)/shard_map/dot_general | solution.py:359
  28.9 0.1 multiply_convert_fusion
  29.0 0.1 select_reduce_fusion
  29.1 0.1 fusion.18
  29.2 0.0 copy-start.4
  29.2 1.2 %copy-done.4 = bf16[256,2048]{1,0:T(8,128)(2,1)S(1)} copy-done((bf16[256,2048]{1,0:T(8,128)(2,1)S(1)}, bf16[256,2048]{1,0:T(8,128)(2,1)}, u32[]{:S(2)}) %copy-start.4) | copy-done | bytes 1048600
  30.4 37.2 %exchange.1 = bf16[16,2048]{1,0:T(8,128)(2,1)S(1)} custom-call(bf16[16,2176]{1,0:T(8,128)(2,1)S(1)} %pad_maximum_fusion.refs_0_, f32[16,2048]{1,0:T(8,128)S(1)} %get-tuple-element.13.refs_1_, f32[1,2048]{1,0:T(1,128)S(1)} %bitcast.18, bf16[2048,256]{1,0:T(8,128)(2,1)S(1)} %copy-done.2, bf16[2048,256]{1,0:T(8,128)(2,1)S(1)} %copy-done.3, ...), custom_call_target="tpu_custom_call" | custom-call | tf_op jit(solution)/shard_map/exchange/pallas_call | solution.py:225
  67.7 0.6 copy.46
  (33 shorter events, 0.1 us)
Async XLA Ops:
  0.0 14.5 %copy-start = (bf16[2048,128]{1,0:T(8,128)(2,1)S(1)}, bf16[2048,128]{1,0:T(8,128)(2,1)}, u32[]{:S(2)}) copy-start(bf16[2048,128]{1,0:T(8,128)(2,1)} %param.25) | copy-start | bytes 1572868
  0.0 4.5 %copy-start.6 = (bf16[16,2048]{1,0:T(8,128)(2,1)S(1)}, bf16[16,2048]{1,0:T(8,128)(2,1)}, u32[]{:S(2)}) copy-start(bf16[16,2048]{1,0:T(8,128)(2,1)} %param.22) | copy-start | bytes 196612
  0.0 4.5 %copy-start.9 = (f32[2048]{0:T(1024)S(1)}, f32[2048]{0:T(1024)}, u32[]{:S(2)}) copy-start(f32[2048]{0:T(1024)} %param.23) | copy-start | bytes 24580
  0.0 4.1 %copy-start.13 = (s32[16]{0:T(128)S(1)}, s32[16]{0:T(128)}, u32[]{:S(2)}) copy-start(s32[16]{0:T(128)} %param.33) | copy-start | bytes 196
  0.0 4.2 %copy-start.8 = (f32[16,2,1024]{2,1,0:T(2,128)S(1)}, f32[16,2,1024]{2,1,0:T(2,128)}, u32[]{:S(2)}) copy-start(f32[16,2,1024]{2,1,0:T(2,128)} %param.32) | copy-start | bytes 393220
  0.0 4.5 %copy-start.14 = (bf16[2048,2]{0,1:T(2,128)(2,1)S(1)}, bf16[2048,2]{0,1:T(2,128)(2,1)}, u32[]{:S(2)}) copy-start(bf16[2048,2]{0,1:T(2,128)(2,1)} %param.27) | copy-start | bytes 24580
  0.0 4.5 %copy-start.15 = (f32[2]{0:T(128)S(1)}, f32[2]{0:T(128)}, u32[]{:S(2)}) copy-start(f32[2]{0:T(128)} %param.28) | copy-start | bytes 28
  11.3 4.0 %copy-start.7 = (bf16[2048,128]{1,0:T(8,128)(2,1)S(1)}, bf16[2048,128]{1,0:T(8,128)(2,1)}, u32[]{:S(2)}) copy-start(bf16[2048,128]{1,0:T(8,128)(2,1)} %param.26) | copy-start | bytes 1572868
  22.1 6.8 %copy-start.10 = (f32[2048]{0:T(1024)S(1)}, f32[2048]{0:T(1024)}, u32[]{:S(2)}) copy-start(f32[2048]{0:T(1024)} %param.34) | copy-start | bytes 24580
  22.1 6.9 %copy-start.11 = (f32[16,4]{0,1:T(4,128)S(1)}, f32[16,4]{0,1:T(4,128)}, u32[]{:S(2)}) copy-start(f32[16,4]{0,1:T(4,128)} %param.43) | copy-start | bytes 772
  22.1 6.9 %copy-start.12 = (s32[16,4]{0,1:T(4,128)S(1)}, s32[16,4]{0,1:T(4,128)}, u32[]{:S(2)}) copy-start(s32[16,4]{0,1:T(4,128)} %param.42) | copy-start | bytes 772
  25.6 3.6 %copy-start.1 = (bf16[1,2048,512]{2,1,0:T(8,128)(2,1)S(1)}, bf16[1,2048,512]{2,1,0:T(8,128)(2,1)}, u32[]{:S(2)}) copy-start(bf16[1,2048,512]{2,1,0:T(8,128)(2,1)} %refs_6_.1) | copy-start | bytes 6291460
  25.6 3.6 %copy-start.5 = (f32[2048]{0:T(1024)S(1)}, f32[2048]{0:T(1024)}, u32[]{:S(2)}) copy-start(f32[2048]{0:T(1024)} %param.35) | copy-start | bytes 24580
  25.7 3.5 %copy-start.2 = (bf16[2048,256]{1,0:T(8,128)(2,1)S(1)}, bf16[2048,256]{1,0:T(8,128)(2,1)}, u32[]{:S(2)}) copy-start(bf16[2048,256]{1,0:T(8,128)(2,1)} %refs_3_.1) | copy-start | bytes 3145732
  25.7 3.5 %copy-start.3 = (bf16[2048,256]{1,0:T(8,128)(2,1)S(1)}, bf16[2048,256]{1,0:T(8,128)(2,1)}, u32[]{:S(2)}) copy-start(bf16[2048,256]{1,0:T(8,128)(2,1)} %refs_4_.1) | copy-start | bytes 3145732
  29.2 1.2 %copy-start.4 = (bf16[256,2048]{1,0:T(8,128)(2,1)S(1)}, bf16[256,2048]{1,0:T(8,128)(2,1)}, u32[]{:S(2)}) copy-start(bf16[256,2048]{1,0:T(8,128)(2,1)} %refs_5_.1) | copy-start | bytes 3145732

commit v2 on v1

--- a/solution.py
+++ b/solution.py
@@ -12,6 +12,7 @@
 CORES = 2
 SIDES = 2
 CHUNKS = 4
+GROUP = 4
 MESH = pl.DeviceIdType.MESH
 
 
@@ -252,70 +253,233 @@
     )(block, residual, branch_gate.reshape(1, -1), *weights)
 
 
-def norm_rows(inputs, gain_vec):
-    widened = inputs.astype(jnp.float32)
-    scaled = widened * lax.rsqrt(jnp.mean(widened * widened, axis=-1, keepdims=True) + EPSILON)
-    return (scaled * gain_vec).astype(jnp.bfloat16)
+def attend_kernel(
+    count,
+    tokens_ref,
+    attn_gain_ref,
+    w_query_hbm,
+    w_key_hbm,
+    w_value_hbm,
+    w_forget_ref,
+    forget_bias_ref,
+    w_attn_out_hbm,
+    keys_hbm,
+    values_hbm,
+    logsum_ref,
+    lengths_ref,
+    ffn_gain_ref,
+    routes_ref,
+    route_weights_ref,
+    residual_ref,
+    block_ref,
+    w_query,
+    w_key,
+    w_value,
+    w_attn_out,
+    keys,
+    values,
+    query_rows,
+    new_keys,
+    new_values,
+    gates,
+    attended_rows,
+    weight_sem,
+    cache_sem,
+):
+    own_rows, width = tokens_ref.shape
+    kv_heads, span = logsum_ref.shape[1:]
+    head_size = w_key.shape[1] // kv_heads
+    scaling = 1.0 / math.sqrt(head_size)
+    pieces = query_rows.shape[1]
+
+    loads = [
+        pltpu.make_async_copy(source, target, weight_sem.at[at])
+        for at, (source, target) in enumerate(
+            (
+                (w_query_hbm, w_query),
+                (w_key_hbm, w_key),
+                (w_value_hbm, w_value),
+                (w_attn_out_hbm, w_attn_out),
+            )
+        )
+    ]
+
+    def cache_loads(at):
+        members = pl.ds(at * GROUP, GROUP)
+        return (
+            pltpu.make_async_copy(keys_hbm.at[members], keys.at[members], cache_sem.at[at, 0]),
+            pltpu.make_async_copy(values_hbm.at[members], values.at[members], cache_sem.at[at, 1]),
+        )
+
+    for load in loads[:3]:
+        load.start()
+    for at in range(own_rows // GROUP):
+        for load in cache_loads(at):
+            load.start()
+    loads[3].start()
+
+    def normalise(widened, gain):
+        mean = jnp.mean(widened * widened, axis=-1, keepdims=True)
+        return (widened * lax.rsqrt(mean + EPSILON) * gain).astype(jnp.bfloat16)
+
+    tokens = tokens_ref[...].astype(jnp.float32)
+    normed = normalise(tokens, attn_gain_ref[...])
+    wide_normed = normed.astype(jnp.float32)
+    for head in range(kv_heads):
+        row = w_forget_ref[pl.ds(head, 1), :].astype(jnp.float32)
+        logit = jnp.sum(wide_normed * row, axis=1, keepdims=True) + forget_bias_ref[head]
+        log_gate = jnp.minimum(logit, 0.0) - jnp.log1p(jnp.exp(-jnp.abs(logit)))
+        gates[:, head, :] = jnp.broadcast_to(log_gate, (own_rows, gates.shape[2]))
+
+    def project(weights):
+        product = jnp.dot(normed, weights[...], preferred_element_type=jnp.float32)
+        return product.astype(jnp.bfloat16).astype(jnp.float32)
+
+    loads[0].wait()
+    queries = project(w_query)
+    for piece in range(pieces):
+        query_rows[:, piece, :] = queries[:, piece * LANES : (piece + 1) * LANES]
+    loads[1].wait()
+    new_keys[...] = project(w_key)
+    loads[2].wait()
+    new_values[...] = project(w_value)
+
+    piece_at = lax.broadcasted_iota(jnp.int32, (pieces, LANES), 0)
+    lane_at = lax.broadcasted_iota(jnp.int32, (pieces, LANES), 1)
+    in_place = (piece_at < pieces // kv_heads) == (lane_at < head_size)
+    row_at = lax.rem(lax.broadcasted_iota(jnp.int32, (2 * pieces, span), 0), pieces)
+    early = row_at < pieces // kv_heads
+    position = lax.broadcasted_iota(jnp.int32, (2 * pieces, span), 1)
+    head_position = lax.broadcasted_iota(jnp.int32, (kv_heads, span), 1)
+
+    def sequence(b):
+        valid = lengths_ref[b]
+        plain = query_rows[b]
+        turned = pltpu.roll(plain, head_size, 1)
+        query = jnp.concatenate(
+            [jnp.where(in_place, plain, 0.0), jnp.where(in_place, turned, 0.0)], axis=0
+        )
+        scores = lax.dot_general(
+            query.astype(jnp.bfloat16),
+            keys[b],
+            (((1,), (1,)), ((), ())),
+            preferred_element_type=jnp.float32,
+        )
+        logsum = logsum_ref[b]
+        latest = jnp.sum(jnp.where(head_position == valid - 1, logsum, 0.0), axis=1, keepdims=True)
+        offsets = (latest + gates[b][:, :1]) - logsum
+        offset = jnp.where(early, offsets[0:1, :], offsets[1:2, :])
+        scores = jnp.where(position < valid, scores * scaling + offset, -jnp.inf)
+        own = jnp.sum(query * new_keys[pl.ds(b, 1), :], axis=1, keepdims=True) * scaling
+        peak = jnp.maximum(jnp.max(scores, axis=1, keepdims=True), own)
+        weight = jnp.exp(scores - peak)
+        own_weight = jnp.exp(own - peak)
+        inverse = 1.0 / (jnp.sum(weight, axis=1, keepdims=True) + own_weight)
+        probs = (weight * inverse).astype(jnp.bfloat16)
+        own_prob = (own_weight * inverse).astype(jnp.bfloat16).astype(jnp.float32)
+        mixed = jnp.dot(probs, values[b], preferred_element_type=jnp.float32)
+        mixed = mixed + own_prob * new_values[pl.ds(b, 1), :]
+        first = jnp.where(in_place, mixed[:pieces], 0.0)
+        other = jnp.where(in_place, mixed[pieces:], 0.0)
+        return first + pltpu.roll(other, head_size, 1)
+
+    def group(at, carried):
+        for load in cache_loads(at):
+            load.wait()
+        results = [sequence(at * GROUP + member) for member in range(GROUP)]
+        for member in range(GROUP):
+            attended_rows[at * GROUP + member] = results[member]
+        return carried
+
+    lax.fori_loop(0, own_rows // GROUP, group, 0)
+
+    attended = jnp.concatenate([attended_rows[:, piece, :] for piece in range(pieces)], axis=1)
+    loads[3].wait()
+    residual = tokens + jnp.dot(
+        attended.astype(jnp.bfloat16), w_attn_out[...], preferred_element_type=jnp.float32
+    )
+    residual_ref[...] = residual
+    block_ref[:, :width] = normalise(residual, ffn_gain_ref[...])
+    lane = lax.broadcasted_iota(jnp.int32, (own_rows, block_ref.shape[1] - width), 1)
+    table = jnp.zeros(lane.shape, jnp.float32)
+    for k in range(routes_ref.shape[1]):
+        chosen = lax.rem(lane, count) == routes_ref[:, k : k + 1]
+        table = table + jnp.where(chosen, route_weights_ref[:, k : k + 1], 0.0)
+    high = table.astype(jnp.bfloat16).astype(jnp.float32)
+    middle = (table - high).astype(jnp.bfloat16).astype(jnp.float32)
+    extra = jnp.where(lane < count, high, jnp.where(lane < 2 * count, middle, table - high - middle))
+    block_ref[:, width:] = extra.astype(jnp.bfloat16)
 
 
 def attend(
-    normed,
+    tokens,
+    attn_gain,
     w_query,
     w_key,
     w_value,
     w_forget,
     forget_bias,
+    w_attn_out,
     cache_keys,
     cache_values,
     cache_logsum,
     lengths,
+    ffn_gain,
+    routes,
+    route_weights,
 ):
-    own_rows = normed.shape[0]
+    count = lax.axis_size("ep")
+    own_rows, width = tokens.shape
     kv_heads = cache_logsum.shape[1]
-    cache_span = cache_logsum.shape[2]
-    head_size = w_key.shape[1] // kv_heads
-    group_size = w_query.shape[1] // head_size // kv_heads
-    scaling = 1.0 / math.sqrt(head_size)
-    queries = jnp.dot(normed, w_query, preferred_element_type=jnp.float32).astype(jnp.bfloat16)
-    new_keys = jnp.dot(normed, w_key, preferred_element_type=jnp.float32).astype(jnp.bfloat16)
-    new_values = jnp.dot(normed, w_value, preferred_element_type=jnp.float32).astype(jnp.bfloat16)
-    log_gate = jax.nn.log_sigmoid(
-        jnp.dot(normed, w_forget, preferred_element_type=jnp.float32) + forget_bias
+    pieces = w_query.shape[1] // LANES
+    wide = width + -(-3 * count // LANES) * LANES
+    bf16, f32 = jnp.bfloat16, jnp.float32
+    near = pl.BlockSpec(memory_space=pltpu.VMEM)
+    far = pl.BlockSpec(memory_space=pl.ANY)
+    scalars = pl.BlockSpec(memory_space=pltpu.SMEM)
+    return pl.pallas_call(
+        lambda *refs: attend_kernel(count, *refs),
+        out_shape=(
+            jax.ShapeDtypeStruct((own_rows, width), f32),
+            jax.ShapeDtypeStruct((own_rows, wide), bf16),
+        ),
+        in_specs=[near, near, far, far, far, near, scalars, far, far, far, near, scalars]
+        + [near, near, near],
+        out_specs=(near, near),
+        scratch_shapes=[
+            pltpu.VMEM(w_query.shape, bf16),
+            pltpu.VMEM(w_key.shape, bf16),
+            pltpu.VMEM(w_value.shape, bf16),
+            pltpu.VMEM(w_attn_out.shape, bf16),
+            pltpu.VMEM(cache_keys.shape, bf16),
+            pltpu.VMEM(cache_values.shape, bf16),
+            pltpu.VMEM((own_rows, pieces, LANES), f32),
+            pltpu.VMEM((own_rows, w_key.shape[1]), f32),
+            pltpu.VMEM((own_rows, w_value.shape[1]), f32),
+            pltpu.VMEM((own_rows, kv_heads, LANES), f32),
+            pltpu.VMEM((own_rows, pieces, LANES), f32),
+            pltpu.SemaphoreType.DMA((4,)),
+            pltpu.SemaphoreType.DMA((own_rows // GROUP, 2)),
+        ],
+        compiler_params=pltpu.CompilerParams(vmem_limit_bytes=40 * 1024 * 1024),
+        name="attend",
+    )(
+        tokens,
+        attn_gain.reshape(1, -1),
+        w_query,
+        w_key,
+        w_value,
+        w_forget.T,
+        forget_bias,
+        w_attn_out,
+        cache_keys,
+        cache_values,
+        cache_logsum,
+        lengths,
+        ffn_gain.reshape(1, -1),
+        routes,
+        route_weights,
     )
-    positions = lax.broadcasted_iota(jnp.int32, (own_rows, kv_heads, cache_span), 2)
-    latest = jnp.sum(jnp.where(positions == lengths[:, None, None] - 1, cache_logsum, 0.0), axis=2)
-    offsets = (latest + log_gate)[:, :, None] - cache_logsum
-    usable = positions < lengths[:, None, None]
-    query_heads = queries.reshape(own_rows, kv_heads, group_size, head_size)
-    key_heads = cache_keys.reshape(own_rows, cache_span, kv_heads, head_size)
-    value_heads = cache_values.reshape(own_rows, cache_span, kv_heads, head_size)
-    scores = (
-        jnp.einsum("bgrd,blgd->bgrl", query_heads, key_heads, preferred_element_type=jnp.float32)
-        * scaling
-    )
-    scores = jnp.where(usable[:, :, None, :], scores + offsets[:, :, None, :], -jnp.inf)
-    self_score = (
-        jnp.einsum(
-            "bgrd,bgd->bgr",
-            query_heads,
-            new_keys.reshape(own_rows, kv_heads, head_size),
-            preferred_element_type=jnp.float32,
-        )
-        * scaling
-    )
-    peak_score = jnp.maximum(jnp.max(scores, axis=3), self_score)
-    cache_weight = jnp.exp(scores - peak_score[..., None])
-    self_weight = jnp.exp(self_score - peak_score)
-    denominator = jnp.sum(cache_weight, axis=3) + self_weight
-    cache_probs = (cache_weight / denominator[..., None]).astype(jnp.bfloat16)
-    self_probs = (self_weight / denominator).astype(jnp.bfloat16)
-    attended = jnp.einsum(
-        "bgrl,blgd->bgrd", cache_probs, value_heads, preferred_element_type=jnp.float32
-    )
-    attended = attended + self_probs.astype(jnp.float32)[..., None] * new_values.reshape(
-        own_rows, kv_heads, 1, head_size
-    ).astype(jnp.float32)
-    return attended.reshape(own_rows, -1).astype(jnp.bfloat16)
 
 
 def body(
@@ -342,33 +506,25 @@
     routes,
     route_weights,
 ):
-    own_rows = tokens.shape[0]
-    normed = norm_rows(tokens, attn_gain)
-    attended = attend(
-        normed,
+    residual, block = attend(
+        tokens,
+        attn_gain,
         w_query,
         w_key,
         w_value,
         w_forget,
         forget_bias,
+        w_attn_out,
         cache_keys,
         cache_values,
         cache_logsum,
         lengths,
+        ffn_gain,
+        routes,
+        route_weights,
     )
-    residual = tokens.astype(jnp.float32) + jnp.dot(
-        attended, w_attn_out, preferred_element_type=jnp.float32
-    )
-    second = norm_rows(residual, ffn_gain)
-    count = lax.axis_size("ep")
-    routed_to = routes[:, :, None] == lax.broadcasted_iota(jnp.int32, routes.shape + (count,), 2)
-    table = jnp.sum(jnp.where(routed_to, route_weights[:, :, None], 0.0), axis=1)
-    high = lax.reduce_precision(table, 8, 7)
-    middle = lax.reduce_precision(table - high, 8, 7)
-    extra = jnp.concatenate([high, middle, table - high - middle], axis=1)
-    extra = jnp.pad(extra, ((0, 0), (0, -extra.shape[1] % LANES))).astype(jnp.bfloat16)
     return exchange(
-        jnp.concatenate([second, extra], axis=1),
+        block,
         residual,
         branch_gate,
         dense_gate,

time: 68.8 us -> 64.7 us (0.940)
  matrix products: 13.4 us -> 0 us
  Pallas kernels: 37.2 us -> 48.1 us
  other arithmetic: 2.16 us -> 0 us
  local copies, waits for them, and re-layouts: 15.3 us -> 16 us
    dot_general x8 -> x0, matrix products: 13.4 us -> none  [the longest x1 3.48 us: attend(): jnp.einsum('bgrl,blgd->bgrd', cache_probs, value_heads, preferred_element...]
    pallas_call x0 -> x1, Pallas kernels: none -> 10.8 us  [attend(): pl.pallas_call(lambda *refs: attend_kernel(count, *refs), out_shape=(jax....]
    reduce_sum x4 -> x0, other arithmetic: 1.65 us -> none  [the longest x1 1.03 us: norm_rows(): jnp.mean(widened * widened, axis=-1, keepdims=True) + EPSILON]
    unnamed x35 -> x37, local copies, waits for them, and re-layouts: 14.7 us -> 16 us
where the time goes in v2:
time: 64.7 us; the launch traced here: 64.1 us
  Pallas kernels  48.1 us (74%)
  local copies, waits for them, and re-layouts  16 us (25%)
    pallas_call x1, Pallas kernels, exchange(): pl.pallas_call(lambda *refs: exchange_kernel(count, depth, *refs), out_sh...  37.3 us
    unnamed x37, local copies, waits for them, and re-layouts  16 us
    pallas_call x1, Pallas kernels, attend(): pl.pallas_call(lambda *refs: attend_kernel(count, *refs), out_shape=(jax....  10.8 us

profile of v2, /device:TPU:0, one launch (start us, length us, event | category | flops | bytes accessed | tf_op | source)
XLA Modules:
  0.0 64.1 jit_solution(14022813536057356236)
XLA Ops:
  0.0 0.8 %copy.23.refs_13_ = s32[16,4]{1,0:T(8,128)S(1)} copy(s32[16,4]{0,1:T(4,128)} %param.42) | data formatting | bytes 512 | tf_op args[20]
  0.8 0.8 %copy.24.refs_14_ = f32[16,4]{1,0:T(8,128)S(1)} copy(f32[16,4]{0,1:T(4,128)} %param.43) | data formatting | bytes 512 | tf_op args[21]
  1.5 0.0 copy-start
  1.5 2.2 %copy-done = bf16[2048,1024]{1,0:T(8,128)(2,1)S(1)} copy-done((bf16[2048,1024]{1,0:T(8,128)(2,1)S(1)}, bf16[2048,1024]{1,0:T(8,128)(2,1)}, u32[]{:S(2)}) %copy-start) | copy-done | bytes 4194328
  3.7 0.0 copy-start.1
  3.7 2.2 %copy-done.1 = bf16[1024,2048]{1,0:T(8,128)(2,1)S(1)} copy-done((bf16[1024,2048]{1,0:T(8,128)(2,1)S(1)}, bf16[1024,2048]{1,0:T(8,128)(2,1)}, u32[]{:S(2)}) %copy-start.1) | copy-done | bytes 4194328
  5.9 0.0 copy-start.2
  5.9 2.2 %copy-done.2 = bf16[16,1024,128]{2,1,0:T(8,128)(2,1)S(1)} copy-done((bf16[16,1024,128]{2,1,0:T(8,128)(2,1)S(1)}, bf16[16,1024,128]{2,1,0:T(8,128)(2,1)}, u32[]{:S(2)}) %copy-start.2) | copy-done | bytes 4194328
  8.1 0.0 copy-start.7
  8.1 1.0 %copy-done.7 = bf16[2048,128]{1,0:T(8,128)(2,1)S(1)} copy-done((bf16[2048,128]{1,0:T(8,128)(2,1)S(1)}, bf16[2048,128]{1,0:T(8,128)(2,1)}, u32[]{:S(2)}) %copy-start.7) | copy-done | bytes 524312
  9.1 0.0 copy-start.8
  9.1 1.0 %copy-done.8 = bf16[2048,128]{1,0:T(8,128)(2,1)S(1)} copy-done((bf16[2048,128]{1,0:T(8,128)(2,1)S(1)}, bf16[2048,128]{1,0:T(8,128)(2,1)}, u32[]{:S(2)}) %copy-start.8) | copy-done | bytes 524312
  10.2 0.0 copy-start.9
  10.2 0.9 %copy-done.9 = f32[16,2,1024]{2,1,0:T(2,128)S(1)} copy-done((f32[16,2,1024]{2,1,0:T(2,128)S(1)}, f32[16,2,1024]{2,1,0:T(2,128)}, u32[]{:S(2)}) %copy-start.9) | copy-done | bytes 131096
  11.1 0.8 %copy-done.10 = bf16[16,2048]{1,0:T(8,128)(2,1)S(1)} copy-done((bf16[16,2048]{1,0:T(8,128)(2,1)S(1)}, bf16[16,2048]{1,0:T(8,128)(2,1)}, u32[]{:S(2)}) %copy-start.10) | copy-done | bytes 65560
  11.9 0.7 %copy-done.11 = f32[2048]{0:T(1024)S(1)} copy-done((f32[2048]{0:T(1024)S(1)}, f32[2048]{0:T(1024)}, u32[]{:S(2)}) %copy-start.11) | copy-done | bytes 8216
  12.6 0.0 copy-start.12
  12.6 0.7 %copy-done.12 = bf16[2048,2]{0,1:T(2,128)(2,1)S(1)} copy-done((bf16[2048,2]{0,1:T(2,128)(2,1)S(1)}, bf16[2048,2]{0,1:T(2,128)(2,1)}, u32[]{:S(2)}) %copy-start.12) | copy-done | bytes 8216
  13.3 0.0 copy-start.13
  13.3 0.7 %copy-done.13 = f32[2048]{0:T(1024)S(1)} copy-done((f32[2048]{0:T(1024)S(1)}, f32[2048]{0:T(1024)}, u32[]{:S(2)}) %copy-start.13) | copy-done | bytes 8216
  14.0 0.0 copy-start.15
  14.0 0.7 %copy-done.15 = f32[2]{0:T(128)S(1)} copy-done((f32[2]{0:T(128)S(1)}, f32[2]{0:T(128)}, u32[]{:S(2)}) %copy-start.15) | copy-done | bytes 32
  14.7 0.7 %copy-done.16 = s32[16]{0:T(128)S(1)} copy-done((s32[16]{0:T(128)S(1)}, s32[16]{0:T(128)}, u32[]{:S(2)}) %copy-start.16) | copy-done | bytes 88
  15.3 0.0 copy-start.14
  15.3 10.8 %attend.1 = (f32[16,2048]{1,0:T(8,128)S(1)}, bf16[16,2176]{1,0:T(8,128)(2,1)S(1)}) custom-call(bf16[16,2048]{1,0:T(8,128)(2,1)S(1)} %copy-done.10, f32[1,2048]{1,0:T(1,128)S(1)} %bitcast.4, bf16[2048,1024]{1,0:T(8,128)(2,1)S(1)} %copy-done, bf16[2048,128]{1,0:T(8,128)(2,1)S(1)} %copy-done.7, bf16[2048,128]{1,0:T(8,128)(2,1)S(1)} %copy-done.8, ...), custom_call_target="tpu_custom_call" | custom-call | tf_op jit(solution)/shard_map/attend/pallas_call | solution.py:440
  26.1 0.0 copy-done.3
  26.2 0.0 copy-done.4
  26.2 0.0 copy-done.5
  26.2 0.0 copy-done.6
  26.2 0.0 copy-done.14
  26.2 37.3 %exchange.1 = bf16[16,2048]{1,0:T(8,128)(2,1)S(1)} custom-call(bf16[16,2176]{1,0:T(8,128)(2,1)S(1)} %get-tuple-element.7.refs_0_, f32[16,2048]{1,0:T(8,128)S(1)} %get-tuple-element.8.refs_1_, f32[1,2048]{1,0:T(1,128)S(1)} %bitcast.7, bf16[2048,256]{1,0:T(8,128)(2,1)S(1)} %copy-done.4, bf16[2048,256]{1,0:T(8,128)(2,1)S(1)} %copy-done.5, ...), custom_call_target="tpu_custom_call" | custom-call | tf_op jit(solution)/shard_map/exchange/pallas_call | solution.py:226
  63.5 0.6 copy.26
  (7 shorter events, 0.0 us)
Async XLA Ops:
  1.5 2.2 %copy-start = (bf16[2048,1024]{1,0:T(8,128)(2,1)S(1)}, bf16[2048,1024]{1,0:T(8,128)(2,1)}, u32[]{:S(2)}) copy-start(bf16[2048,1024]{1,0:T(8,128)(2,1)} %refs_2_.1) | copy-start | bytes 12582916
  3.7 2.2 %copy-start.1 = (bf16[1024,2048]{1,0:T(8,128)(2,1)S(1)}, bf16[1024,2048]{1,0:T(8,128)(2,1)}, u32[]{:S(2)}) copy-start(bf16[1024,2048]{1,0:T(8,128)(2,1)} %refs_7_.2) | copy-start | bytes 12582916
  5.9 2.2 %copy-start.2 = (bf16[16,1024,128]{2,1,0:T(8,128)(2,1)S(1)}, bf16[16,1024,128]{2,1,0:T(8,128)(2,1)}, u32[]{:S(2)}) copy-start(bf16[16,1024,128]{2,1,0:T(8,128)(2,1)} %refs_8_.2) | copy-start | bytes 12582916
  8.1 1.0 %copy-start.7 = (bf16[2048,128]{1,0:T(8,128)(2,1)S(1)}, bf16[2048,128]{1,0:T(8,128)(2,1)}, u32[]{:S(2)}) copy-start(bf16[2048,128]{1,0:T(8,128)(2,1)} %refs_3_.2) | copy-start | bytes 1572868
  9.1 1.0 %copy-start.8 = (bf16[2048,128]{1,0:T(8,128)(2,1)S(1)}, bf16[2048,128]{1,0:T(8,128)(2,1)}, u32[]{:S(2)}) copy-start(bf16[2048,128]{1,0:T(8,128)(2,1)} %refs_4_.2) | copy-start | bytes 1572868
  10.2 0.9 %copy-start.9 = (f32[16,2,1024]{2,1,0:T(2,128)S(1)}, f32[16,2,1024]{2,1,0:T(2,128)}, u32[]{:S(2)}) copy-start(f32[16,2,1024]{2,1,0:T(2,128)} %refs_10_.1) | copy-start | bytes 393220
  11.1 0.8 %copy-start.10 = (bf16[16,2048]{1,0:T(8,128)(2,1)S(1)}, bf16[16,2048]{1,0:T(8,128)(2,1)}, u32[]{:S(2)}) copy-start(bf16[16,2048]{1,0:T(8,128)(2,1)} %refs_0_.1) | copy-start | bytes 196612
  11.9 0.7 %copy-start.11 = (f32[2048]{0:T(1024)S(1)}, f32[2048]{0:T(1024)}, u32[]{:S(2)}) copy-start(f32[2048]{0:T(1024)} %param.23) | copy-start | bytes 24580
  12.6 0.7 %copy-start.12 = (bf16[2048,2]{0,1:T(2,128)(2,1)S(1)}, bf16[2048,2]{0,1:T(2,128)(2,1)}, u32[]{:S(2)}) copy-start(bf16[2048,2]{0,1:T(2,128)(2,1)} %param.27) | copy-start | bytes 24580
  13.3 0.7 %copy-start.13 = (f32[2048]{0:T(1024)S(1)}, f32[2048]{0:T(1024)}, u32[]{:S(2)}) copy-start(f32[2048]{0:T(1024)} %param.34) | copy-start | bytes 24580
  14.0 0.7 %copy-start.15 = (f32[2]{0:T(128)S(1)}, f32[2]{0:T(128)}, u32[]{:S(2)}) copy-start(f32[2]{0:T(128)} %refs_6_.2) | copy-start | bytes 28
  14.7 0.7 %copy-start.16 = (s32[16]{0:T(128)S(1)}, s32[16]{0:T(128)}, u32[]{:S(2)}) copy-start(s32[16]{0:T(128)} %refs_11_.1) | copy-start | bytes 196
  15.3 10.8 %copy-start.3 = (bf16[1,2048,512]{2,1,0:T(8,128)(2,1)S(1)}, bf16[1,2048,512]{2,1,0:T(8,128)(2,1)}, u32[]{:S(2)}) copy-start(bf16[1,2048,512]{2,1,0:T(8,128)(2,1)} %refs_6_.3) | copy-start | bytes 6291460
  15.3 10.8 %copy-start.4 = (bf16[2048,256]{1,0:T(8,128)(2,1)S(1)}, bf16[2048,256]{1,0:T(8,128)(2,1)}, u32[]{:S(2)}) copy-start(bf16[2048,256]{1,0:T(8,128)(2,1)} %refs_3_.3) | copy-start | bytes 3145732
  15.3 10.9 %copy-start.5 = (bf16[2048,256]{1,0:T(8,128)(2,1)S(1)}, bf16[2048,256]{1,0:T(8,128)(2,1)}, u32[]{:S(2)}) copy-start(bf16[2048,256]{1,0:T(8,128)(2,1)} %refs_4_.3) | copy-start | bytes 3145732
  15.3 10.9 %copy-start.6 = (bf16[256,2048]{1,0:T(8,128)(2,1)S(1)}, bf16[256,2048]{1,0:T(8,128)(2,1)}, u32[]{:S(2)}) copy-start(bf16[256,2048]{1,0:T(8,128)(2,1)} %refs_5_.1) | copy-start | bytes 3145732
  15.3 10.9 %copy-start.14 = (f32[2048]{0:T(1024)S(1)}, f32[2048]{0:T(1024)}, u32[]{:S(2)}) copy-start(f32[2048]{0:T(1024)} %param.35) | copy-start | bytes 24580

commit v3 on v2

--- a/solution.py
+++ b/solution.py
@@ -11,8 +11,9 @@
 LANES = 128
 CORES = 2
 SIDES = 2
-CHUNKS = 4
-GROUP = 4
+CHUNKS = 2
+GROUP = 8
+VMEM_BYTES = 67043328
 MESH = pl.DeviceIdType.MESH
 
 
@@ -121,10 +122,10 @@
     def pass_on(source, slot, at, peer):
         send(source, slot, gather_send.at[at], gather_recv.at[at], peer)
 
+    pass_on(block_ref, own_slot, side_at, across)
+    pass_on(block_ref, own_slot, core_at, partner)
     for d in range(1, depth):
         pass_on(block_ref, own_slot, d - 1, device(away(d), side, core))
-    pass_on(block_ref, own_slot, side_at, across)
-    pass_on(block_ref, own_slot, core_at, partner)
     rows_buf[core, side, level] = block_ref[...]
     for d in range(1, depth + 1):
         if d < depth:
@@ -135,6 +136,22 @@
         slot = rows_buf.at[core, 1 - side, behind(d - 1)]
         arrive(slot, gather_recv.at[side_at + d - 1])
         pass_on(slot, slot, core_at + depth + d - 1, partner)
+    for load in loads[:4]:
+        load.wait()
+
+    def hidden(group, gate_ref, up_ref):
+        rows = rows_buf[group].reshape(count // CORES * own_rows, block_ref.shape[1])[:, :width]
+        gate_part = jnp.dot(rows, gate_ref[...], preferred_element_type=jnp.float32)
+        up_part = jnp.dot(rows, up_ref[...], preferred_element_type=jnp.float32)
+        return jax.nn.silu(gate_part) * up_part
+
+    def in_order(near, distant):
+        ahead = jnp.where(core == 0, near, distant)
+        after = jnp.where(core == 0, distant, near)
+        return jnp.concatenate([ahead, after], axis=0).astype(jnp.bfloat16)
+
+    near_dense = hidden(core, dense_gate, dense_up)
+    near_expert = hidden(core, expert_gate, expert_up)
     for d in range(depth):
         arrive(rows_buf.at[1 - core, side, behind(d)], gather_recv.at[core_at + d])
     for d in range(depth):
@@ -150,17 +167,8 @@
         jnp.sum(second.astype(jnp.float32) * branch_ref[...], axis=1, keepdims=True)
     )
 
-    def hidden(gate_ref, up_ref):
-        gate_part = jnp.dot(second, gate_ref[...], preferred_element_type=jnp.float32)
-        up_part = jnp.dot(second, up_ref[...], preferred_element_type=jnp.float32)
-        return (jax.nn.silu(gate_part) * up_part).astype(jnp.bfloat16)
-
-    loads[0].wait()
-    loads[1].wait()
-    dense_hidden = hidden(dense_gate, dense_up)
-    loads[2].wait()
-    loads[3].wait()
-    expert_hidden = hidden(expert_gate, expert_up)
+    dense_hidden = in_order(near_dense, hidden(1 - core, dense_gate, dense_up))
+    expert_hidden = in_order(near_expert, hidden(1 - core, expert_gate, expert_up))
     loads[4].wait()
     loads[5].wait()
 
@@ -247,7 +255,7 @@
             pltpu.SemaphoreType.DMA((CHUNKS, scatters)),
         ],
         compiler_params=pltpu.CompilerParams(
-            collective_id=0, has_side_effects=True, vmem_limit_bytes=48 * 1024 * 1024
+            collective_id=0, has_side_effects=True, vmem_limit_bytes=VMEM_BYTES
         ),
         name="exchange",
     )(block, residual, branch_gate.reshape(1, -1), *weights)
@@ -283,6 +291,7 @@
     new_values,
     gates,
     attended_rows,
+    extra_rows,
     weight_sem,
     cache_sem,
 ):
@@ -317,6 +326,19 @@
         for load in cache_loads(at):
             load.start()
     loads[3].start()
+
+    lane = lax.broadcasted_iota(jnp.int32, (1, extra_rows.shape[1]), 1)
+    expert = lax.rem(lane, count)
+    for b in range(own_rows):
+        table = jnp.zeros(lane.shape, jnp.float32)
+        for k in range(routes_ref.shape[0]):
+            table = table + jnp.where(expert == routes_ref[k, b], route_weights_ref[k, b], 0.0)
+        high = table.astype(jnp.bfloat16).astype(jnp.float32)
+        middle = (table - high).astype(jnp.bfloat16).astype(jnp.float32)
+        low = table - high - middle
+        extra_rows[b : b + 1, :] = jnp.where(
+            lane < count, high, jnp.where(lane < 2 * count, middle, low)
+        )
 
     def normalise(widened, gain):
         mean = jnp.mean(widened * widened, axis=-1, keepdims=True)
@@ -400,15 +422,7 @@
     )
     residual_ref[...] = residual
     block_ref[:, :width] = normalise(residual, ffn_gain_ref[...])
-    lane = lax.broadcasted_iota(jnp.int32, (own_rows, block_ref.shape[1] - width), 1)
-    table = jnp.zeros(lane.shape, jnp.float32)
-    for k in range(routes_ref.shape[1]):
-        chosen = lax.rem(lane, count) == routes_ref[:, k : k + 1]
-        table = table + jnp.where(chosen, route_weights_ref[:, k : k + 1], 0.0)
-    high = table.astype(jnp.bfloat16).astype(jnp.float32)
-    middle = (table - high).astype(jnp.bfloat16).astype(jnp.float32)
-    extra = jnp.where(lane < count, high, jnp.where(lane < 2 * count, middle, table - high - middle))
-    block_ref[:, width:] = extra.astype(jnp.bfloat16)
+    block_ref[:, width:] = extra_rows[...].astype(jnp.bfloat16)
 
 
 def attend(
@@ -444,7 +458,7 @@
             jax.ShapeDtypeStruct((own_rows, wide), bf16),
         ),
         in_specs=[near, near, far, far, far, near, scalars, far, far, far, near, scalars]
-        + [near, near, near],
+        + [near, scalars, scalars],
         out_specs=(near, near),
         scratch_shapes=[
             pltpu.VMEM(w_query.shape, bf16),
@@ -458,10 +472,11 @@
             pltpu.VMEM((own_rows, w_value.shape[1]), f32),
             pltpu.VMEM((own_rows, kv_heads, LANES), f32),
             pltpu.VMEM((own_rows, pieces, LANES), f32),
+            pltpu.VMEM((own_rows, wide - width), f32),
             pltpu.SemaphoreType.DMA((4,)),
             pltpu.SemaphoreType.DMA((own_rows // GROUP, 2)),
         ],
-        compiler_params=pltpu.CompilerParams(vmem_limit_bytes=40 * 1024 * 1024),
+        compiler_params=pltpu.CompilerParams(vmem_limit_bytes=VMEM_BYTES),
         name="attend",
     )(
         tokens,
@@ -477,8 +492,8 @@
         cache_logsum,
         lengths,
         ffn_gain.reshape(1, -1),
-        routes,
-        route_weights,
+        routes.T,
+        route_weights.T,
     )
 
 

time: 64.7 us -> 49.9 us (0.77)
  local copies, waits for them, and re-layouts: 16 us -> 1.47 us
    unnamed x37 -> x1, local copies, waits for them, and re-layouts: 16 us -> 1.47 us
    pallas_call x1, Pallas kernels: 10.8 us -> 13 us  [attend(): pl.pallas_call(lambda *refs: attend_kernel(count, *refs), out_shape=(jax....]
    pallas_call x1, Pallas kernels: 37.3 us -> 35.1 us  [exchange(): pl.pallas_call(lambda *refs: exchange_kernel(count, depth, *refs), out_sh...]
where the time goes in v3:
time: 49.9 us; the launch traced here: 49.7 us
  Pallas kernels  48.2 us (97%)
  local copies, waits for them, and re-layouts  1.47 us (3%)
    pallas_call x1, Pallas kernels, exchange(): pl.pallas_call(lambda *refs: exchange_kernel(count, depth, *refs), out_sh...  35.1 us
    pallas_call x1, Pallas kernels, attend(): pl.pallas_call(lambda *refs: attend_kernel(count, *refs), out_shape=(jax....  13 us
    unnamed x1, local copies, waits for them, and re-layouts  1.47 us

profile of v3, /device:TPU:0, one launch (start us, length us, event | category | flops | bytes accessed | tf_op | source)
XLA Modules:
  0.0 49.7 jit_solution(13334565266006511479)
XLA Ops:
  0.0 13.0 %attend.1 = (f32[16,2048]{1,0:T(8,128)}, bf16[16,2176]{1,0:T(8,128)(2,1)}) custom-call(bf16[16,2048]{1,0:T(8,128)(2,1)} %refs_0_.1, f32[1,2048]{1,0:T(1,128)} %bitcast.6, bf16[2048,1024]{1,0:T(8,128)(2,1)} %refs_2_.1, bf16[2048,128]{1,0:T(8,128)(2,1)} %refs_3_.2, bf16[2048,128]{1,0:T(8,128)(2,1)} %refs_4_.2, bf16[2,2048]{1,0:T(2,128)(2,1)} %bitcast.7, ...), custom_call_target="tpu_custom_call" | custom-call | tf_op jit(solution)/shard_map/attend/pallas_call | solution.py:454
  13.0 35.1 %exchange.1 = bf16[16,2048]{1,0:T(8,128)(2,1)} custom-call(bf16[16,2176]{1,0:T(8,128)(2,1)} %get-tuple-element.7.refs_0_, f32[16,2048]{1,0:T(8,128)} %get-tuple-element.8.refs_1_, f32[1,2048]{1,0:T(1,128)} %bitcast.9, bf16[2048,256]{1,0:T(8,128)(2,1)} %refs_3_.3, bf16[2048,256]{1,0:T(8,128)(2,1)} %refs_4_.3, bf16[256,2048]{1,0:T(8,128)(2,1)} %refs_5_.1, ...), custom_call_target="tpu_custom_call" | custom-call | tf_op jit(solution)/shard_map/exchange/pallas_call | solution.py:234
  48.2 1.5 %copy.24 = bf16[16,2048]{1,0:T(8,128)(2,1)} copy(bf16[16,2048]{1,0:T(8,128)(2,1)} %exchange.1) | data formatting | bytes 131072
